TPU v7x, 32 devices: a whole 2x2x4 slice. The times are simulated.
32 devices in a mesh: sp: 4 (over z), fs: 4 (over y, x), tp: 2 (over core).
Axes of the slice: x: 2, y: 2, z: 4, core: 2. Of those that a mesh axis runs over, the one named last changes fastest.
Arguments:
- activations: bfloat16 [4, 1024, 2048], P('fs', 'sp'), may hold values from -600 to 600
- norm_gain: float32 [2048], replicated, may hold values from 0.1 to 1.9
- w_conv_gate: bfloat16 [2048, 1024], P('sp', ('fs', 'tp')), may hold values from -0.125 to 0.125
- w_conv_mult: bfloat16 [2048, 1024], P('sp', ('fs', 'tp')), may hold values from -0.125 to 0.125
- w_conv_in: bfloat16 [2048, 1024], P('sp', ('fs', 'tp')), may hold values from -0.125 to 0.125
- conv_taps: float32 [3, 1024], replicated, may hold values from -3.5 to 3.5
- w_query: bfloat16 [2048, 1024], P('sp', ('fs', 'tp')), may hold values from -0.125 to 0.125
- w_key: bfloat16 [2048, 1024], P('sp', ('fs', 'tp')), may hold values from -0.125 to 0.125
- w_value: bfloat16 [2048, 1024], P('sp', ('fs', 'tp')), may hold values from -0.125 to 0.125
- w_input_gate: bfloat16 [2048, 8], replicated, may hold values from -0.125 to 0.125
- w_forget_gate: bfloat16 [2048, 8], replicated, may hold values from -0.125 to 0.125
- gate_bias: float32 [2, 8], replicated, may hold values from -1 to 120
- decay_shift: float32 [4, 1024, 8], P(None, 'sp'), may hold values from -2 to 0, as said below
- head_gain: float32 [1024], replicated, may hold values from 0.1 to 1.9
- w_out_conv: bfloat16 [1024, 2048], P(('fs', 'tp'), 'sp'), may hold values from -0.125 to 0.125
- w_out_mem: bfloat16 [1024, 2048], P(('fs', 'tp'), 'sp'), may hold values from -0.125 to 0.125
Outputs:
- output: bfloat16 [4, 1024, 2048], P('fs', ('sp', 'tp'))
Inputs may be any that keep to these rules, and one draw needn't show every extreme that they name: `decay_shift`: never positive.
All inputs are finite; a program needn't handle non-finite values.
Results may differ from a plain program's by a relative error of at most 0.015.
Values may be sent and summed in bfloat16 or wider, within the bound.
A program may use at most 64 MiB of HBM per device.

v0:
```python
import jax
import jax.numpy as jnp
from jax import lax
from jax.sharding import PartitionSpec as P

MEMORY_HEADS = 8
HEAD_DIM = 128
BLOCK = 64
EPSILON = 1e-06
FAR_BELOW = -1e30
HIGHEST_PRECISION = lax.Precision.HIGHEST


def prefix(value, axis, join, neutral):
    count, mine = (lax.axis_size(axis), lax.axis_index(axis))
    pieces = jax.tree.map(lambda part: lax.all_gather(part, axis), value)
    subtotal = jax.tree.map(
        lambda part, zero: jnp.full_like(part, 0) + jnp.asarray(zero, part.dtype), value, neutral
    )

    def lap(position, subtotal):
        longer = join(subtotal, jax.tree.map(lambda part: part[position], pieces))
        return jax.tree.map(lambda new, old: jnp.where(position < mine, new, old), longer, subtotal)

    return lax.fori_loop(0, count - 1, lap, subtotal)


def from_behind(array, axis, by):
    peers = lax.axis_size(axis)
    pairs = [(i, i + by) for i in range(peers) if 0 <= i + by < peers]
    return lax.ppermute(array, axis, pairs)


def combine_states(earlier, later):
    total_one, peak_one, state_one = earlier
    total_two, peak_two, state_two = later
    peak_new = jnp.maximum(total_two + peak_one, peak_two)
    scale_old = jnp.exp(total_two + peak_one - peak_new)
    scale_new = jnp.exp(peak_two - peak_new)
    return (
        total_one + total_two,
        peak_new,
        scale_old[..., None, None] * state_one + scale_new[..., None, None] * state_two,
    )


def head_rows(values, seq_count, heads_here):
    tokens = values.shape[1]
    split_heads = values.reshape(seq_count, tokens, heads_here, HEAD_DIM).transpose(0, 2, 1, 3)
    return split_heads.reshape(seq_count * heads_here, tokens, HEAD_DIM).astype(jnp.float32)


def gate_rows(values, seq_count, heads_here):
    tokens = values.shape[1]
    return values.transpose(0, 2, 1).reshape(seq_count * heads_here, tokens)


def memory_cell(query_rows, key_rows, value_rows, entry_gate, log_forget):
    members = query_rows.shape[0]
    tokens = query_rows.shape[1]
    head_width = query_rows.shape[2]
    nblocks = tokens // BLOCK
    block_shape = (members, nblocks, BLOCK, head_width)
    query_blocks = query_rows.reshape(block_shape)
    key_blocks = key_rows.reshape(block_shape) * head_width ** (-0.5)
    value_blocks = value_rows.reshape(block_shape)
    entry_blocks = entry_gate.reshape(members, nblocks, BLOCK)
    forget_sums = jnp.cumsum(log_forget.reshape(members, nblocks, BLOCK), axis=-1)
    block_total = forget_sums[..., -1]
    local_logs = block_total[..., None] - forget_sums + entry_blocks
    local_peak = jnp.max(local_logs, axis=-1)
    local_weights = jnp.exp(local_logs - local_peak[..., None])
    local_state = jnp.einsum(
        "bclv,bclk->bcvk",
        local_weights[..., None] * value_blocks,
        key_blocks,
        precision=HIGHEST_PRECISION,
    )

    def advance(running, block_item):
        return (combine_states(running, block_item), running)

    zero_sums = jnp.zeros((members,), jnp.float32)
    low_peaks = jnp.full((members,), FAR_BELOW, jnp.float32)
    zero_states = jnp.zeros((members, head_width, head_width), jnp.float32)
    block_items = (
        jnp.moveaxis(block_total, 1, 0),
        jnp.moveaxis(local_peak, 1, 0),
        jnp.moveaxis(local_state, 1, 0),
    )
    device_total, inner_states = lax.scan(advance, (zero_sums, low_peaks, zero_states), block_items)
    inner_states = tuple((jnp.moveaxis(tensor, 0, 1) for tensor in inner_states))
    total_sum, total_peak, total_state = device_total
    before = prefix(
        (total_sum, total_peak, total_state),
        "sp",
        combine_states,
        (zero_sums, low_peaks, zero_states),
    )
    opening = combine_states((zero_sums, zero_sums, zero_states), before)
    opening = tuple((tensor[:, None] for tensor in opening))
    _, prior_peak, prior_state = combine_states(opening, inner_states)
    positions = jnp.arange(BLOCK)
    causal_mask = positions[:, None] >= positions[None, :]
    pair_logs = jnp.where(
        causal_mask,
        forget_sums[..., :, None] - forget_sums[..., None, :] + entry_blocks[..., None, :],
        -jnp.inf,
    )
    carried_logs = forget_sums + prior_peak[..., None]
    row_peak = jnp.maximum(carried_logs, jnp.max(pair_logs, axis=-1))
    inner_weights = jnp.exp(pair_logs - row_peak[..., None])
    carried_weights = jnp.exp(carried_logs - row_peak)
    scores = inner_weights * jnp.einsum(
        "bcld,bcsd->bcls", query_blocks, key_blocks, precision=HIGHEST_PRECISION
    )
    numerator = carried_weights[..., None] * jnp.einsum(
        "bcvk,bclk->bclv", prior_state, query_blocks, precision=HIGHEST_PRECISION
    ) + jnp.einsum("bcls,bcsv->bclv", scores, value_blocks, precision=HIGHEST_PRECISION)
    return numerator.reshape(members, tokens, head_width)


def shards(
    activations,
    norm_gain,
    w_conv_gate,
    w_conv_mult,
    w_conv_in,
    conv_taps,
    w_query,
    w_key,
    w_value,
    w_input_gate,
    w_forget_gate,
    gate_bias,
    decay_shift,
    head_gain,
    w_out_conv,
    w_out_mem,
):
    group_index = lax.axis_index(("fs", "tp"))
    heads_here = MEMORY_HEADS // (lax.axis_size("fs") * lax.axis_size("tp"))
    channels = w_conv_gate.shape[1]
    sequences = lax.all_gather(activations, "fs", axis=0, tiled=True)
    seq_count = sequences.shape[0]
    tokens = sequences.shape[1]
    model_width = sequences.shape[2]
    row_count = seq_count * tokens
    flat_rows = sequences.reshape(row_count, model_width).astype(jnp.float32)
    normed = (
        flat_rows
        * lax.rsqrt(jnp.mean(flat_rows * flat_rows, axis=-1, keepdims=True) + EPSILON)
        * norm_gain
    ).astype(jnp.bfloat16)
    pieces = (
        lax.all_gather(w_conv_gate, "sp", axis=0, tiled=True),
        lax.all_gather(w_conv_mult, "sp", axis=0, tiled=True),
        lax.all_gather(w_conv_in, "sp", axis=0, tiled=True),
        lax.all_gather(w_query, "sp", axis=0, tiled=True),
        lax.all_gather(w_key, "sp", axis=0, tiled=True),
        lax.all_gather(w_value, "sp", axis=0, tiled=True),
    )
    projected = tuple(
        (jnp.dot(normed, shard_piece, preferred_element_type=jnp.float32) for shard_piece in pieces)
    )
    conv_gate, conv_mult, conv_in, query, keys_proj, value = [
        tensor.astype(jnp.bfloat16).reshape(seq_count, tokens, -1) for tensor in projected
    ]
    product = (conv_mult.astype(jnp.float32) * conv_in.astype(jnp.float32)).astype(jnp.bfloat16)
    ntaps = conv_taps.shape[0]
    rim_rows = from_behind(product[:, tokens - (ntaps - 1) :, :], "sp", 1)
    padded = jnp.concatenate([rim_rows, product], axis=1).astype(jnp.float32)
    tap_weights = lax.dynamic_slice_in_dim(conv_taps, group_index * channels, channels, 1)
    mixed_sum = jnp.zeros((seq_count, tokens, channels), jnp.float32)
    for tap_index in range(ntaps):
        mixed_sum = (
            mixed_sum + tap_weights[tap_index] * padded[:, tap_index : tap_index + tokens, :]
        )
    conv_out = (conv_gate.astype(jnp.float32) * mixed_sum).astype(jnp.bfloat16)
    entry_cols = lax.dynamic_slice_in_dim(w_input_gate, group_index * heads_here, heads_here, 1)
    forget_cols = lax.dynamic_slice_in_dim(w_forget_gate, group_index * heads_here, heads_here, 1)
    gate_values = jnp.dot(
        normed,
        jnp.concatenate([entry_cols, forget_cols], axis=1),
        preferred_element_type=jnp.float32,
    ).reshape(seq_count, tokens, 2 * heads_here)
    bias_rows = lax.dynamic_slice_in_dim(gate_bias, group_index * heads_here, heads_here, 1)
    decay_rows = lax.dynamic_slice_in_dim(decay_shift, group_index * heads_here, heads_here, 2)
    entry = gate_values[..., :heads_here] + bias_rows[0]
    log_forget = jax.nn.log_sigmoid(gate_values[..., heads_here:] + bias_rows[1]) + decay_rows
    cell = memory_cell(
        head_rows(query, seq_count, heads_here),
        head_rows(keys_proj, seq_count, heads_here),
        head_rows(value, seq_count, heads_here),
        gate_rows(entry, seq_count, heads_here),
        gate_rows(log_forget, seq_count, heads_here),
    )
    cell = cell * lax.rsqrt(jnp.mean(cell * cell, axis=-1, keepdims=True) + EPSILON)
    gain_rows = lax.dynamic_slice_in_dim(
        head_gain, group_index * heads_here * HEAD_DIM, heads_here * HEAD_DIM, 0
    ).reshape(1, heads_here, 1, HEAD_DIM)
    scaled = cell.reshape(seq_count, heads_here, tokens, HEAD_DIM) * gain_rows
    mem_out = (
        scaled.transpose(0, 2, 1, 3)
        .reshape(seq_count, tokens, heads_here * HEAD_DIM)
        .astype(jnp.bfloat16)
    )
    conv_seq, mem_seq = (
        lax.all_to_all(conv_out, "fs", split_axis=0, concat_axis=2, tiled=True),
        lax.all_to_all(mem_out, "fs", split_axis=0, concat_axis=2, tiled=True),
    )
    rows_conv, rows_mem = (
        lax.all_gather(w_out_conv, "fs", axis=0, tiled=True),
        lax.all_gather(w_out_mem, "fs", axis=0, tiled=True),
    )
    full_conv, full_mem = (
        lax.all_gather(rows_conv, "sp", axis=1, tiled=True),
        lax.all_gather(rows_mem, "sp", axis=1, tiled=True),
    )
    conv_flat = conv_seq[0]
    mem_flat = mem_seq[0]
    output = lax.psum_scatter(
        (
            jnp.dot(conv_flat, full_conv, preferred_element_type=jnp.float32)
            + jnp.dot(mem_flat, full_mem, preferred_element_type=jnp.float32)
        ).astype(jnp.bfloat16),
        "tp",
        scatter_dimension=0,
        tiled=True,
    ).astype(jnp.float32)
    return output.astype(jnp.bfloat16).reshape(1, output.shape[0], -1)


def solution(mesh):
    return jax.shard_map(
        shards,
        mesh=mesh,
        in_specs=(
            P("fs", "sp", None),
            P(),
            P("sp", ("fs", "tp")),
            P("sp", ("fs", "tp")),
            P("sp", ("fs", "tp")),
            P(),
            P("sp", ("fs", "tp")),
            P("sp", ("fs", "tp")),
            P("sp", ("fs", "tp")),
            P(),
            P(),
            P(),
            P(None, "sp", None),
            P(),
            P(("fs", "tp"), "sp"),
            P(("fs", "tp"), "sp"),
        ),
        out_specs=P("fs", ("sp", "tp"), None),
        check_vma=False,
    )
```

profile of v0, /device:TPU:0, one launch (start us, length us, event | category | flops | bytes accessed | tf_op | source)
XLA Modules:
  0.0 249.8 jit_solution(10992935933422332303)
XLA Ops:
  8.7 17.6 %all_gather.58 = bf16[2048,128]{1,0:T(8,128)(2,1)S(1)} all-gather(bf16[512,128]{1,0:T(8,128)(2,1)} %param.27), channel_id=1, replica_groups=mesh['sp'=4,'fs'=4,'tp'=2] {'sp'}, dimensions={0}, use_global_device_ids=true | all-gather | bytes 655360 | tf_op jit(solution)/shard_map/all_gather | solution.py:160
  26.3 16.6 %all_gather.57 = bf16[2048,128]{1,0:T(8,128)(2,1)S(1)} all-gather(bf16[512,128]{1,0:T(8,128)(2,1)} %param.28), channel_id=1, replica_groups=mesh['sp'=4,'fs'=4,'tp'=2] {'sp'}, dimensions={0}, use_global_device_ids=true | all-gather | bytes 655360 | tf_op jit(solution)/shard_map/all_gather | solution.py:161
  43.7 20.8 %all-gather.8.cloned.1.call-done = bf16[4,256,2048]{2,1,0:T(8,128)(2,1)} async-done(((bf16[1,256,2048]{2,1,0:T(8,128)(2,1)}), bf16[4,256,2048]{2,1,0:T(8,128)(2,1)}) %all-gather.8.cloned.1.call-update) | async-done | bytes 4194320 | tf_op jit(solution)/shard_map/all_gather | solution.py:144
  64.5 3.2 %multiply_reduce_fusion = f32[4,256]{1,0:T(4,128)S(1)} fusion(bf16[4,256,2048]{2,1,0:T(8,128)(2,1)} %all-gather.8.cloned.1.call-done), kind=kLoop, calls=%fused_computation.34 | loop fusion | flops 6290432 | bytes 4198400 | tf_op jit(solution)/shard_map/reduce_sum | solution.py:152
  69.2 2.2 fusion.43
  72.9 3.2 %fusion.14 = bf16[1024,2048]{1,0:T(8,128)(2,1)S(1)} fusion(bf16[4,256,2048]{2,1,0:T(8,128)(2,1)} %all-gather.8.cloned.1.call-done, f32[2048]{0:T(1024)S(1)} %copy-done.8, f32[1024]{0:T(1024)S(1)} %bitcast.163), kind=kLoop, calls=%fused_computation.32 | loop fusion | flops 8388608 | bytes 8400896 | tf_op jit(solution)/shard_map/convert_element_type | solution.py:154
  78.8 2.0 convolution_bitcast_fusion
  82.7 10.6 %all_gather.55 = bf16[512,512]{1,0:T(8,128)(2,1)} all-gather(bf16[128,512]{1,0:T(8,128)(2,1)S(1)} %copy-done.6), channel_id=1, replica_groups=mesh['sp'=4,'fs'=4,'tp'=2] {'fs'}, dimensions={0}, use_global_device_ids=true | all-gather | bytes 655360 | tf_op jit(solution)/shard_map/all_gather | solution.py:213
  93.4 10.4 %all_gather.66 = bf16[512,512]{1,0:T(8,128)(2,1)} all-gather(bf16[128,512]{1,0:T(8,128)(2,1)S(1)} %copy-done.7), channel_id=1, replica_groups=mesh['sp'=4,'fs'=4,'tp'=2] {'fs'}, dimensions={0}, use_global_device_ids=true | all-gather | bytes 655360 | tf_op jit(solution)/shard_map/all_gather | solution.py:214
  103.9 19.9 %all_gather.65 = bf16[2048,128]{1,0:T(8,128)(2,1)} all-gather(bf16[512,128]{1,0:T(8,128)(2,1)} %param.26), channel_id=1, replica_groups=mesh['sp'=4,'fs'=4,'tp'=2] {'sp'}, dimensions={0}, use_global_device_ids=true | all-gather | bytes 655360 | tf_op jit(solution)/shard_map/all_gather | solution.py:159
  123.8 20.8 %all_gather.53 = bf16[2048,128]{1,0:T(8,128)(2,1)S(1)} all-gather(bf16[512,128]{1,0:T(8,128)(2,1)} %param.23), channel_id=1, replica_groups=mesh['sp'=4,'fs'=4,'tp'=2] {'sp'}, dimensions={0}, use_global_device_ids=true | all-gather | bytes 655360 | tf_op jit(solution)/shard_map/all_gather | solution.py:157
  144.6 20.7 %all_gather.54 = bf16[2048,128]{1,0:T(8,128)(2,1)S(1)} all-gather(bf16[512,128]{1,0:T(8,128)(2,1)} %param.24), channel_id=1, replica_groups=mesh['sp'=4,'fs'=4,'tp'=2] {'sp'}, dimensions={0}, use_global_device_ids=true | all-gather | bytes 655360 | tf_op jit(solution)/shard_map/all_gather | solution.py:158
  166.3 20.4 %all_gather.52 = bf16[2048,128]{1,0:T(8,128)(2,1)} all-gather(bf16[512,128]{1,0:T(8,128)(2,1)} %param.22), channel_id=1, replica_groups=mesh['sp'=4,'fs'=4,'tp'=2] {'sp'}, dimensions={0}, use_global_device_ids=true | all-gather | bytes 655360 | tf_op jit(solution)/shard_map/all_gather | solution.py:156
  187.9 4.3 %convolution_convert_fusion = bf16[1024,128]{1,0:T(8,128)(2,1)} fusion(bf16[1024,2048]{1,0:T(8,128)(2,1)} %copy-done.1, bf16[2048,128]{1,0:T(8,128)(2,1)} %all_gather.65), kind=kOutput, calls=%fused_computation.45 | convolution fusion | flops 537001984 | bytes 4980736 | tf_op jit(solution)/shard_map/dot_general | solution.py:164
  195.0 2.1 collective-permute-start
  197.1 3.6 %convolution_convert_fusion.5 = bf16[1024,128]{1,0:T(8,128)(2,1)S(1)} fusion(bf16[1024,2048]{1,0:T(8,128)(2,1)} %copy-done.1, bf16[2048,128]{1,0:T(8,128)(2,1)} %all_gather.52), kind=kOutput, calls=%fused_computation.56 | convolution fusion | flops 537001984 | bytes 4980736 | tf_op jit(solution)/shard_map/dot_general | solution.py:164
  201.5 10.3 %all-reduce.2 = (f32[16]{0:T(128)S(1)}, f32[16]{0:T(128)S(1)}) all-reduce(f32[16]{0:T(128)S(1)} %dynamic-update-slice, f32[16]{0:T(128)S(1)} %dynamic-update-slice.1), channel_id=2, replica_groups=mesh['sp'=4,'fs'=4,'tp'=2] {'sp'}, use_global_device_ids=true, to_apply=%add | all-reduce | flops 32 | bytes 256
  213.5 3.4 %all-to-all-start = ((bf16[4,256,128]{1,2,0:T(8,128)(2,1)}), bf16[4,256,128]{1,2,0:T(8,128)(2,1)S(1)}, u32[]{:S(2)}, u32[]{:S(2)}) async-start(bf16[4,256,128]{1,2,0:T(8,128)(2,1)} %fusion.31), calls=%async_computation | async-start | bytes 524288 | tf_op jit(solution)/shard_map/all_to_all | solution.py:209
  216.9 3.4 %while.40 = (s32[]{:T(128)}, f32[4]{0:T(128)S(1)}, f32[4]{0:T(128)S(1)}, f32[4,128,128]{2,1,0:T(8,128)S(1)}, s32[]{:T(128)}, /*index=5*/f32[4,4]{1,0:T(4,128)S(1...) while((s32[]{:T(128)}, f32[4]{0:T(128)S(1)}, f32[4]{0:T(128)S(1)}, ...), condition=%wide.region_6.7_spmd.clone, body=%wide.region_5.6_spmd.clone.sunk | while | flops 327728 | bytes 786793 | solution.py:25
  224.1 4.1 %all-to-all-start.1 = ((bf16[4,256,128]{1,2,0:T(8,128)(2,1)}), bf16[4,256,128]{1,2,0:T(8,128)(2,1)S(1)}, u32[]{:S(2)}, u32[]{:S(2)}) async-start(bf16[4,256,128]{1,2,0:T(8,128)(2,1)} %multiply_convert_fusion.2), calls=%async_computation.1 | async-start | bytes 524288 | tf_op jit(solution)/shard_map/all_to_all | solution.py:210
  228.2 2.3 fusion.52
  230.5 3.0 %all-to-all-done.1 = bf16[4,256,128]{1,2,0:T(8,128)(2,1)S(1)} async-done(((bf16[4,256,128]{1,2,0:T(8,128)(2,1)}), bf16[4,256,128]{1,2,0:T(8,128)(2,1)S(1)}, u32[]{:S(2)}, u32[]{:S(2)}) %all-to-all-start.1) | async-done | bytes 262176 | tf_op jit(solution)/shard_map/all_to_all | solution.py:210
  233.5 3.3 %fusion.19 = bf16[256,2048]{1,0:T(8,128)(2,1)} fusion(f32[256,2048]{1,0:T(8,128)S(1)} %fusion.52, bf16[256,512]{0,1:T(8,128)(2,1)S(1)} %bitcast.159, bf16[512,2048]{1,0:T(8,128)(2,1)} %all-gather.12.cloned.1.call-done), kind=kOutput, calls=%fused_computation.40 | convolution fusion | flops 537919488 | bytes 5505024 | tf_op jit(solution)/shard_map/dot_general | solution.py:225
  236.9 6.4 %reduce-scatter.2.cloned.1.call-done = bf16[128,2048]{1,0:T(8,128)(2,1)} async-done(((bf16[256,2048]{1,0:T(8,128)(2,1)}), bf16[128,2048]{1,0:T(8,128)(2,1)}) %reduce-scatter.2.cloned.1.call-update) | async-done | bytes 524304 | tf_op jit(solution)/shard_map/reduce_scatter | solution.py:222
  (127 shorter events, 25.2 us)
Async XLA Ops:
  6.5 159.7 %copy-start = (f32[3,1024]{1,0:T(4,128)S(1)}, f32[3,1024]{1,0:T(4,128)}, u32[]{:S(2)}) copy-start(f32[3,1024]{1,0:T(4,128)} %param.25) | copy-start | bytes 36868
  6.5 61.2 %copy-start.8 = (f32[2048]{0:T(1024)S(1)}, f32[2048]{0:T(1024)}, u32[]{:S(2)}) copy-start(f32[2048]{0:T(1024)} %param.21) | copy-start | bytes 24580
  6.5 58.0 %all-gather.8.cloned.1.call-start = ((), (), s32[]{:S(2)}) async-start(), calls=%async_computation.3 | async-start | bytes 5242880 | tf_op jit(solution)/shard_map/all_gather | solution.py:144
  7.3 209.7 %all-gather.14.cloned.1.call-start = ((), (), s32[]{:S(2)}) async-start(), calls=%async_computation.7 | async-start | bytes 1310720 | tf_op jit(solution)/shard_map/all_gather | solution.py:16
  64.5 3.4 %copy-start.4 = (bf16[4,256,2048]{2,1,0:T(8,128)(2,1)S(1)}, bf16[4,256,2048]{2,1,0:T(8,128)(2,1)}, u32[]{:S(2)}) copy-start(bf16[4,256,2048]{2,1,0:T(8,128)(2,1)} %all-gather.8.cloned.1.call-done) | copy-start | bytes 12582916
  76.1 2.5 %copy-start.1 = (bf16[1024,2048]{1,0:T(8,128)(2,1)}, bf16[1024,2048]{1,0:T(8,128)(2,1)S(1)}, u32[]{:S(2)}) copy-start(bf16[1024,2048]{1,0:T(8,128)(2,1)S(1)} %fusion.14) | copy-start | bytes 12582916
  78.8 3.8 %copy-start.6 = (bf16[128,512]{1,0:T(8,128)(2,1)S(1)}, bf16[128,512]{1,0:T(8,128)(2,1)}, u32[]{:S(2)}) copy-start(bf16[128,512]{1,0:T(8,128)(2,1)} %param.34) | copy-start | bytes 393220
  80.8 12.6 %copy-start.7 = (bf16[128,512]{1,0:T(8,128)(2,1)S(1)}, bf16[128,512]{1,0:T(8,128)(2,1)}, u32[]{:S(2)}) copy-start(bf16[128,512]{1,0:T(8,128)(2,1)} %param.35) | copy-start | bytes 393220
  81.9 0.7 copy-start.3
  81.9 104.8 %copy-start.9 = (u32[32]{0:T(128)S(1)}, u32[32]{0:T(128)}, u32[]{:S(2)}) copy-start(u32[32]{0:T(128)} %constant.88) | copy-start | bytes 388
  82.6 145.5 %all-gather.10.cloned.1.call-start = ((), (), s32[]{:S(2)}) async-start(), calls=%async_computation.4 | async-start | bytes 2621440 | tf_op jit(solution)/shard_map/all_gather | solution.py:217
  93.3 137.2 %all-gather.12.cloned.1.call-start = ((), (), s32[]{:S(2)}) async-start(), calls=%async_computation.5 | async-start | bytes 2621440 | tf_op jit(solution)/shard_map/all_gather | solution.py:218
  165.3 26.9 %copy-start.2 = (bf16[1024,2048]{1,0:T(8,128)(2,1)S(1)}, bf16[1024,2048]{1,0:T(8,128)(2,1)}, u32[]{:S(2)}) copy-start(bf16[1024,2048]{1,0:T(8,128)(2,1)} %copy-done.1) | copy-start | bytes 12582916
  195.0 17.2 %collective-permute-start = (bf16[4,2,128]{1,2,0:T(8,128)(2,1)S(1)}, bf16[4,2,128]{1,2,0:T(8,128)(2,1)S(1)}, u32[]{:S(2)}, u32[]{:S(2)}) collective-permute-start(bf16[4,2,128]{1,2,0:T(8,128)(2,1)S(1)} %slice.48), channel_id=1, source_target_pairs={{0,8},{8,16},{16,24},{1,9},{9,17},{17,25},{2,10},{10,18},{18,26},{... | collective-permute-start | bytes 6152 | tf_op jit(solution)/shard_map/ppermute | solution.py:31
  212.2 8.5 %copy-start.5 = (bf16[1024,128]{1,0:T(8,128)(2,1)S(1)}, bf16[1024,128]{1,0:T(8,128)(2,1)}, u32[]{:S(2)}) copy-start(bf16[1024,128]{1,0:T(8,128)(2,1)} %convolution_convert_fusion) | copy-start | bytes 786436
  213.5 10.6 %all-to-all-start = ((bf16[4,256,128]{1,2,0:T(8,128)(2,1)}), bf16[4,256,128]{1,2,0:T(8,128)(2,1)S(1)}, u32[]{:S(2)}, u32[]{:S(2)}) async-start(bf16[4,256,128]{1,2,0:T(8,128)(2,1)} %fusion.31), calls=%async_computation | async-start | bytes 524288 | tf_op jit(solution)/shard_map/all_to_all | solution.py:209
  224.1 9.5 %all-to-all-start.1 = ((bf16[4,256,128]{1,2,0:T(8,128)(2,1)}), bf16[4,256,128]{1,2,0:T(8,128)(2,1)S(1)}, u32[]{:S(2)}, u32[]{:S(2)}) async-start(bf16[4,256,128]{1,2,0:T(8,128)(2,1)} %multiply_convert_fusion.2), calls=%async_computation.1 | async-start | bytes 524288 | tf_op jit(solution)/shard_map/all_to_all | solution.py:210
  228.2 15.1 %reduce-scatter.2.cloned.1.call-start = ((), (), s32[]{:S(2)}) async-start(), calls=%async_computation.6 | async-start | bytes 1572864 | tf_op jit(solution)/shard_map/reduce_scatter | solution.py:222
Sparse Core Ops, SparseCore 0:
  9.2 55.2 all-gather.7
  82.8 31.4 all-gather.13
  115.9 67.3 all-gather.9
  184.7 44.9 all-gather.11
  237.0 6.2 reduce-scatter.1
where the time goes:
time: 251 us; the launch traced here: 250 us
  blocking collectives  147 us (59%)
  waiting for transfers between devices  31.1 us (12%)
  matrix products  24 us (10%)
  other arithmetic  16.5 us (7%)
  between operations  14.2 us (6%)
  starting transfers between devices  9.73 us (4%)
  local copies, waits for them, and re-layouts  6.76 us (3%)
    all_gather x1, waiting for transfers between devices, shards(): sequences = lax.all_gather(activations, 'fs', axis=0, tiled=True)  20.8 us
    all_gather x1, blocking collectives, shards(): lax.all_gather(w_conv_mult, 'sp', axis=0, tiled=True)  20.8 us
    all_gather x1, blocking collectives, shards(): lax.all_gather(w_conv_in, 'sp', axis=0, tiled=True)  20.7 us
    all_gather x1, blocking collectives, shards(): lax.all_gather(w_conv_gate, 'sp', axis=0, tiled=True)  20.4 us
    all_gather x1, blocking collectives, shards(): lax.all_gather(w_query, 'sp', axis=0, tiled=True)  19.9 us
    all_gather x1, blocking collectives, shards(): lax.all_gather(w_key, 'sp', axis=0, tiled=True)  17.6 us
    all_gather x1, blocking collectives, shards(): lax.all_gather(w_value, 'sp', axis=0, tiled=True)  16.6 us
    dot_general x6, matrix products, shards(): jnp.dot(normed, shard_piece, preferred_element_type=jnp.float32)  12.9 us
  transfers between devices with their start and end apart: 8, of which 3 were waited for; matrix products, arithmetic and copies ran while one was open for 10% of the time, Pallas kernels for 0%

commit v1 on v0

--- a/solution.py
+++ b/solution.py
@@ -2,6 +2,7 @@
 import jax.numpy as jnp
 from jax import lax
 from jax.sharding import PartitionSpec as P
+from jax.lax import all_to_all, axis_size
 
 MEMORY_HEADS = 8
 HEAD_DIM = 128
@@ -9,6 +10,15 @@
 EPSILON = 1e-06
 FAR_BELOW = -1e30
 HIGHEST_PRECISION = lax.Precision.HIGHEST
+
+
+def prepare_teams_all(local_values):
+    return jnp.concatenate(
+        all_to_all(
+            jnp.stack(axis_size("sp") * [local_values]), axis_name="sp", split_axis=0, concat_axis=0
+        ),
+        axis=0,
+    )
 
 
 def prefix(value, axis, join, neutral):
@@ -158,7 +168,7 @@
         lax.all_gather(w_conv_in, "sp", axis=0, tiled=True),
         lax.all_gather(w_query, "sp", axis=0, tiled=True),
         lax.all_gather(w_key, "sp", axis=0, tiled=True),
-        lax.all_gather(w_value, "sp", axis=0, tiled=True),
+        prepare_teams_all(w_value),
     )
     projected = tuple(
         (jnp.dot(normed, shard_piece, preferred_element_type=jnp.float32) for shard_piece in pieces)

time: 251 us -> 260 us (1.036)
  blocking collectives: 147 us -> 136 us
  starting transfers between devices: 9.73 us -> 16 us
  matrix products: 24 us -> 28.3 us
  local copies, waits for them, and re-layouts: 6.76 us -> 10.5 us
  waiting for transfers between devices: 31.1 us -> 34.4 us
  other arithmetic: 16.5 us -> 19.4 us
    all_gather x1 -> x0, blocking collectives: 16.6 us -> none  [shards(): lax.all_gather(w_value, 'sp', axis=0, tiled=True)]
    all_to_all x0 -> x1, starting transfers between devices: none -> 6.35 us  [prepare_teams_all(): all_to_all(jnp.stack(axis_size('sp') * [local_values]), axis_name='sp', s...]
    all_gather x1, blocking collectives: 17.6 us -> 22.8 us  [shards(): lax.all_gather(w_key, 'sp', axis=0, tiled=True)]
    dot_general x6, matrix products: 12.9 us -> 17.2 us  [shards(): jnp.dot(normed, shard_piece, preferred_element_type=jnp.float32)]
    all_gather x1, waiting for transfers between devices: 20.8 us -> 24.1 us  [shards(): sequences = lax.all_gather(activations, 'fs', axis=0, tiled=True)]
    convert_element_type x1 -> x2, other arithmetic: 3.2 us -> 6.19 us  [shards(): normed = (flat_rows * lax.rsqrt(jnp.mean(flat_rows * flat_rows, axis=-1,...]
  transfers between devices with their start and end apart: 8 -> 9, of which waited for: 3 -> 3; matrix products, arithmetic and copies ran while one was open for 10% -> 18% of each run, Pallas kernels for 0% -> 0%
where the time goes in v1:
time: 260 us; the launch traced here: 259 us
  blocking collectives  136 us (52%)
  waiting for transfers between devices  34.4 us (13%)
  matrix products  28.3 us (11%)
  other arithmetic  19.4 us (7%)
  starting transfers between devices  16 us (6%)
  between operations  14.2 us (5%)
  local copies, waits for them, and re-layouts  10.5 us (4%)
    all_gather x1, waiting for transfers between devices, shards(): sequences = lax.all_gather(activations, 'fs', axis=0, tiled=True)  24.1 us
    all_gather x1, blocking collectives, shards(): lax.all_gather(w_key, 'sp', axis=0, tiled=True)  22.8 us
    all_gather x1, blocking collectives, shards(): lax.all_gather(w_conv_mult, 'sp', axis=0, tiled=True)  20.8 us
    all_gather x1, blocking collectives, shards(): lax.all_gather(w_conv_in, 'sp', axis=0, tiled=True)  20.7 us
    all_gather x1, blocking collectives, shards(): lax.all_gather(w_conv_gate, 'sp', axis=0, tiled=True)  20.5 us
    all_gather x1, blocking collectives, shards(): lax.all_gather(w_query, 'sp', axis=0, tiled=True)  19.9 us
    dot_general x6, matrix products, shards(): jnp.dot(normed, shard_piece, preferred_element_type=jnp.float32)  17.2 us
    all_gather x1, blocking collectives, shards(): lax.all_gather(w_out_conv, 'fs', axis=0, tiled=True)  10.6 us
  transfers between devices with their start and end apart: 9, of which 3 were waited for; matrix products, arithmetic and copies ran while one was open for 18% of the time, Pallas kernels for 0%

profile of v1, /device:TPU:0, one launch (start us, length us, event | category | flops | bytes accessed | tf_op | source)
XLA Modules:
  0.0 258.9 jit_solution(7497748061594863083)
XLA Ops:
  9.0 6.3 %all-to-all-start.1 = ((bf16[4,512,128]{2,1,0:T(8,128)(2,1)}), bf16[4,512,128]{2,1,0:T(8,128)(2,1)S(1)}, u32[]{:S(2)}, u32[]{:S(2)}) async-start(bf16[4,512,128]{2,1,0:T(8,128)(2,1)} %stack.2), calls=%async_computation.1 | async-start | bytes 1048576 | tf_op jit(solution)/shard_map/all_to_all | solution.py:17
  16.8 22.8 %all_gather.54 = bf16[2048,128]{1,0:T(8,128)(2,1)S(1)} all-gather(bf16[512,128]{1,0:T(8,128)(2,1)} %param.27), channel_id=1, replica_groups=mesh['sp'=4,'fs'=4,'tp'=2] {'sp'}, dimensions={0}, use_global_device_ids=true | all-gather | bytes 655360 | tf_op jit(solution)/shard_map/all_gather | solution.py:170
  40.4 24.1 %all-gather.8.cloned.1.call-done = bf16[4,256,2048]{2,1,0:T(8,128)(2,1)} async-done(((bf16[1,256,2048]{2,1,0:T(8,128)(2,1)}), bf16[4,256,2048]{2,1,0:T(8,128)(2,1)}) %all-gather.8.cloned.1.call-update) | async-done | bytes 4194320 | tf_op jit(solution)/shard_map/all_gather | solution.py:154
  64.5 3.2 %multiply_reduce_fusion = f32[4,256]{1,0:T(4,128)S(1)} fusion(bf16[4,256,2048]{2,1,0:T(8,128)(2,1)} %all-gather.8.cloned.1.call-done), kind=kLoop, calls=%fused_computation.34 | loop fusion | flops 6290432 | bytes 4198400 | tf_op jit(solution)/shard_map/reduce_sum | solution.py:162
  75.3 5.2 %fusion.14 = bf16[1024,2048]{1,0:T(8,128)(2,1)} fusion(bf16[4,256,2048]{2,1,0:T(8,128)(2,1)} %all-gather.8.cloned.1.call-done, f32[2048]{0:T(1024)S(1)} %copy-done.8, f32[1024]{0:T(1024)S(1)} %bitcast.168), kind=kLoop, calls=%fused_computation.32 | loop fusion | flops 8388608 | bytes 8400896 | tf_op jit(solution)/shard_map/convert_element_type | solution.py:164
  81.1 3.4 %fusion.18 = f32[1024,128]{1,0:T(8,128)S(1)} fusion(bf16[1024,2048]{1,0:T(8,128)(2,1)} %fusion.14, bf16[2048,128]{1,0:T(8,128)(2,1)S(1)} %all_gather.54), kind=kOutput, calls=%fused_computation.44 | convolution fusion | flops 537264128 | bytes 5242880 | tf_op jit(solution)/shard_map/dot_general | solution.py:174
  84.5 3.4 %convolution_convert_fusion.2 = bf16[1024,128]{1,0:T(8,128)(2,1)S(1)} fusion(bf16[1024,2048]{1,0:T(8,128)(2,1)} %bitcast.152, bf16[2048,128]{1,0:T(8,128)(2,1)S(1)} %bitcast.164), kind=kOutput, calls=%fused_computation.45 | convolution fusion | flops 537001984 | bytes 4980736 | tf_op jit(solution)/shard_map/dot_general | solution.py:174
  91.8 10.6 %all_gather.52 = bf16[512,512]{1,0:T(8,128)(2,1)} all-gather(bf16[128,512]{1,0:T(8,128)(2,1)S(1)} %copy-done.6), channel_id=1, replica_groups=mesh['sp'=4,'fs'=4,'tp'=2] {'fs'}, dimensions={0}, use_global_device_ids=true | all-gather | bytes 655360 | tf_op jit(solution)/shard_map/all_gather | solution.py:223
  102.5 10.5 %all_gather.62 = bf16[512,512]{1,0:T(8,128)(2,1)} all-gather(bf16[128,512]{1,0:T(8,128)(2,1)S(1)} %copy-done.7), channel_id=1, replica_groups=mesh['sp'=4,'fs'=4,'tp'=2] {'fs'}, dimensions={0}, use_global_device_ids=true | all-gather | bytes 655360 | tf_op jit(solution)/shard_map/all_gather | solution.py:224
  113.1 19.9 %all_gather.61 = bf16[2048,128]{1,0:T(8,128)(2,1)} all-gather(bf16[512,128]{1,0:T(8,128)(2,1)} %param.26), channel_id=1, replica_groups=mesh['sp'=4,'fs'=4,'tp'=2] {'sp'}, dimensions={0}, use_global_device_ids=true | all-gather | bytes 655360 | tf_op jit(solution)/shard_map/all_gather | solution.py:169
  133.0 20.8 %all_gather.50 = bf16[2048,128]{1,0:T(8,128)(2,1)S(1)} all-gather(bf16[512,128]{1,0:T(8,128)(2,1)} %param.23), channel_id=1, replica_groups=mesh['sp'=4,'fs'=4,'tp'=2] {'sp'}, dimensions={0}, use_global_device_ids=true | all-gather | bytes 655360 | tf_op jit(solution)/shard_map/all_gather | solution.py:167
  153.8 20.7 %all_gather.51 = bf16[2048,128]{1,0:T(8,128)(2,1)S(1)} all-gather(bf16[512,128]{1,0:T(8,128)(2,1)} %param.24), channel_id=1, replica_groups=mesh['sp'=4,'fs'=4,'tp'=2] {'sp'}, dimensions={0}, use_global_device_ids=true | all-gather | bytes 655360 | tf_op jit(solution)/shard_map/all_gather | solution.py:168
  175.4 20.5 %all_gather.49 = bf16[2048,128]{1,0:T(8,128)(2,1)} all-gather(bf16[512,128]{1,0:T(8,128)(2,1)} %param.22), channel_id=1, replica_groups=mesh['sp'=4,'fs'=4,'tp'=2] {'sp'}, dimensions={0}, use_global_device_ids=true | all-gather | bytes 655360 | tf_op jit(solution)/shard_map/all_gather | solution.py:166
  197.1 4.3 %convolution_convert_fusion = bf16[1024,128]{1,0:T(8,128)(2,1)} fusion(bf16[1024,2048]{1,0:T(8,128)(2,1)} %fusion.14, bf16[2048,128]{1,0:T(8,128)(2,1)} %all_gather.61), kind=kOutput, calls=%fused_computation.41 | convolution fusion | flops 537001984 | bytes 4980736 | tf_op jit(solution)/shard_map/dot_general | solution.py:174
  204.1 2.1 collective-permute-start
  206.2 3.6 %convolution_convert_fusion.5 = bf16[1024,128]{1,0:T(8,128)(2,1)S(1)} fusion(bf16[1024,2048]{1,0:T(8,128)(2,1)} %fusion.14, bf16[2048,128]{1,0:T(8,128)(2,1)} %all_gather.49), kind=kOutput, calls=%fused_computation.52 | convolution fusion | flops 537001984 | bytes 4980736 | tf_op jit(solution)/shard_map/dot_general | solution.py:174
  210.7 10.3 %all-reduce.2 = (f32[16]{0:T(128)S(1)}, f32[16]{0:T(128)S(1)}) all-reduce(f32[16]{0:T(128)S(1)} %dynamic-update-slice, f32[16]{0:T(128)S(1)} %dynamic-update-slice.1), channel_id=2, replica_groups=mesh['sp'=4,'fs'=4,'tp'=2] {'sp'}, use_global_device_ids=true, to_apply=%add | all-reduce | flops 32 | bytes 256
  222.6 3.4 %all-to-all-start = ((bf16[4,256,128]{1,2,0:T(8,128)(2,1)}), bf16[4,256,128]{1,2,0:T(8,128)(2,1)S(1)}, u32[]{:S(2)}, u32[]{:S(2)}) async-start(bf16[4,256,128]{1,2,0:T(8,128)(2,1)} %fusion.27), calls=%async_computation | async-start | bytes 524288 | tf_op jit(solution)/shard_map/all_to_all | solution.py:219
  226.0 3.4 %while.40 = (s32[]{:T(128)}, f32[4]{0:T(128)S(1)}, f32[4]{0:T(128)S(1)}, f32[4,128,128]{2,1,0:T(8,128)S(1)}, s32[]{:T(128)}, /*index=5*/f32[4,4]{1,0:T(4,128)S(1...) while((s32[]{:T(128)}, f32[4]{0:T(128)S(1)}, f32[4]{0:T(128)S(1)}, ...), condition=%wide.region_6.7_spmd.clone, body=%wide.region_5.6_spmd.clone.sunk | while | flops 327728 | bytes 786793 | solution.py:35
  233.2 4.1 %all-to-all-start.2 = ((bf16[4,256,128]{1,2,0:T(8,128)(2,1)}), bf16[4,256,128]{1,2,0:T(8,128)(2,1)S(1)}, u32[]{:S(2)}, u32[]{:S(2)}) async-start(bf16[4,256,128]{1,2,0:T(8,128)(2,1)} %multiply_convert_fusion.1), calls=%async_computation.2 | async-start | bytes 524288 | tf_op jit(solution)/shard_map/all_to_all | solution.py:220
  237.3 2.3 fusion.49
  239.6 3.0 %all-to-all-done.2 = bf16[4,256,128]{1,2,0:T(8,128)(2,1)S(1)} async-done(((bf16[4,256,128]{1,2,0:T(8,128)(2,1)}), bf16[4,256,128]{1,2,0:T(8,128)(2,1)S(1)}, u32[]{:S(2)}, u32[]{:S(2)}) %all-to-all-start.2) | async-done | bytes 262176 | tf_op jit(solution)/shard_map/all_to_all | solution.py:220
  242.6 3.3 %fusion.15 = bf16[256,2048]{1,0:T(8,128)(2,1)} fusion(f32[256,2048]{1,0:T(8,128)S(1)} %fusion.49, bf16[256,512]{0,1:T(8,128)(2,1)S(1)} %bitcast.163, bf16[512,2048]{1,0:T(8,128)(2,1)} %all-gather.12.cloned.1.call-done), kind=kOutput, calls=%fused_computation.36 | convolution fusion | flops 537919488 | bytes 5505024 | tf_op jit(solution)/shard_map/dot_general | solution.py:235
  246.0 6.4 %reduce-scatter.2.cloned.1.call-done = bf16[128,2048]{1,0:T(8,128)(2,1)} async-done(((bf16[256,2048]{1,0:T(8,128)(2,1)}), bf16[128,2048]{1,0:T(8,128)(2,1)}) %reduce-scatter.2.cloned.1.call-update) | async-done | bytes 524304 | tf_op jit(solution)/shard_map/reduce_scatter | solution.py:232
  (130 shorter events, 31.4 us)
Async XLA Ops:
  6.5 168.8 %copy-start = (f32[3,1024]{1,0:T(4,128)S(1)}, f32[3,1024]{1,0:T(4,128)}, u32[]{:S(2)}) copy-start(f32[3,1024]{1,0:T(4,128)} %param.25) | copy-start | bytes 36868
  6.5 61.2 %copy-start.8 = (f32[2048]{0:T(1024)S(1)}, f32[2048]{0:T(1024)}, u32[]{:S(2)}) copy-start(f32[2048]{0:T(1024)} %param.21) | copy-start | bytes 24580
  6.5 58.0 %all-gather.8.cloned.1.call-start = ((), (), s32[]{:S(2)}) async-start(), calls=%async_computation.4 | async-start | bytes 5242880 | tf_op jit(solution)/shard_map/all_gather | solution.py:154
  9.0 75.5 %all-to-all-start.1 = ((bf16[4,512,128]{2,1,0:T(8,128)(2,1)}), bf16[4,512,128]{2,1,0:T(8,128)(2,1)S(1)}, u32[]{:S(2)}, u32[]{:S(2)}) async-start(bf16[4,512,128]{2,1,0:T(8,128)(2,1)} %stack.2), calls=%async_computation.1 | async-start | bytes 1048576 | tf_op jit(solution)/shard_map/all_to_all | solution.py:17
  15.4 210.7 %all-gather.14.cloned.1.call-start = ((), (), s32[]{:S(2)}) async-start(), calls=%async_computation.8 | async-start | bytes 1310720 | tf_op jit(solution)/shard_map/all_gather | solution.py:26
  64.5 3.4 %copy-start.2 = (bf16[4,256,2048]{2,1,0:T(8,128)(2,1)S(1)}, bf16[4,256,2048]{2,1,0:T(8,128)(2,1)}, u32[]{:S(2)}) copy-start(bf16[4,256,2048]{2,1,0:T(8,128)(2,1)} %all-gather.8.cloned.1.call-done) | copy-start | bytes 12582916
  69.0 2.0 copy-start.4
  88.0 3.9 %copy-start.6 = (bf16[128,512]{1,0:T(8,128)(2,1)S(1)}, bf16[128,512]{1,0:T(8,128)(2,1)}, u32[]{:S(2)}) copy-start(bf16[128,512]{1,0:T(8,128)(2,1)} %param.34) | copy-start | bytes 393220
  90.0 12.6 %copy-start.7 = (bf16[128,512]{1,0:T(8,128)(2,1)S(1)}, bf16[128,512]{1,0:T(8,128)(2,1)}, u32[]{:S(2)}) copy-start(bf16[128,512]{1,0:T(8,128)(2,1)} %param.35) | copy-start | bytes 393220
  91.1 0.7 copy-start.3
  91.1 104.8 %copy-start.9 = (u32[32]{0:T(128)S(1)}, u32[32]{0:T(128)}, u32[]{:S(2)}) copy-start(u32[32]{0:T(128)} %constant.88) | copy-start | bytes 388
  91.8 145.5 %all-gather.10.cloned.1.call-start = ((), (), s32[]{:S(2)}) async-start(), calls=%async_computation.5 | async-start | bytes 2621440 | tf_op jit(solution)/shard_map/all_gather | solution.py:227
  102.5 137.1 %all-gather.12.cloned.1.call-start = ((), (), s32[]{:S(2)}) async-start(), calls=%async_computation.6 | async-start | bytes 2621440 | tf_op jit(solution)/shard_map/all_gather | solution.py:228
  174.4 26.9 %copy-start.1 = (bf16[1024,2048]{1,0:T(8,128)(2,1)S(1)}, bf16[1024,2048]{1,0:T(8,128)(2,1)}, u32[]{:S(2)}) copy-start(bf16[1024,2048]{1,0:T(8,128)(2,1)} %fusion.14) | copy-start | bytes 12582916
  204.1 17.2 %collective-permute-start = (bf16[4,2,128]{1,2,0:T(8,128)(2,1)S(1)}, bf16[4,2,128]{1,2,0:T(8,128)(2,1)S(1)}, u32[]{:S(2)}, u32[]{:S(2)}) collective-permute-start(bf16[4,2,128]{1,2,0:T(8,128)(2,1)S(1)} %slice.48), channel_id=1, source_target_pairs={{0,8},{8,16},{16,24},{1,9},{9,17},{17,25},{2,10},{10,18},{18,26},{... | collective-permute-start | bytes 6152 | tf_op jit(solution)/shard_map/ppermute | solution.py:41
  221.3 8.5 %copy-start.5 = (bf16[1024,128]{1,0:T(8,128)(2,1)S(1)}, bf16[1024,128]{1,0:T(8,128)(2,1)}, u32[]{:S(2)}) copy-start(bf16[1024,128]{1,0:T(8,128)(2,1)} %convolution_convert_fusion) | copy-start | bytes 786436
  222.6 10.6 %all-to-all-start = ((bf16[4,256,128]{1,2,0:T(8,128)(2,1)}), bf16[4,256,128]{1,2,0:T(8,128)(2,1)S(1)}, u32[]{:S(2)}, u32[]{:S(2)}) async-start(bf16[4,256,128]{1,2,0:T(8,128)(2,1)} %fusion.27), calls=%async_computation | async-start | bytes 524288 | tf_op jit(solution)/shard_map/all_to_all | solution.py:219
  233.2 9.5 %all-to-all-start.2 = ((bf16[4,256,128]{1,2,0:T(8,128)(2,1)}), bf16[4,256,128]{1,2,0:T(8,128)(2,1)S(1)}, u32[]{:S(2)}, u32[]{:S(2)}) async-start(bf16[4,256,128]{1,2,0:T(8,128)(2,1)} %multiply_convert_fusion.1), calls=%async_computation.2 | async-start | bytes 524288 | tf_op jit(solution)/shard_map/all_to_all | solution.py:220
  237.3 15.1 %reduce-scatter.2.cloned.1.call-start = ((), (), s32[]{:S(2)}) async-start(), calls=%async_computation.7 | async-start | bytes 1572864 | tf_op jit(solution)/shard_map/reduce_scatter | solution.py:232
Sparse Core Ops, SparseCore 0:
  9.2 55.2 all-gather.7
  91.9 31.4 all-gather.13
  125.0 67.3 all-gather.9
  193.9 44.9 all-gather.11
  246.1 6.2 reduce-scatter.1
